TPU v7x, 32 devices: a whole 2x2x4 slice. The times are simulated.
32 devices in a mesh: rep: 2 (over y), fs: 4 (over z), tp: 4 (over x, core).
Axes of the slice: x: 2, y: 2, z: 4, core: 2. Of those that a mesh axis runs over, the one named last changes fastest.
Arguments:
- tokens: bfloat16 [4096, 2048], P(('rep', 'fs', 'tp')), may hold values from -6 to 6
- norm_gain: float32 [2048], replicated, may hold values from 0.1 to 1.9
- w_gate: bfloat16 [2048, 3072], P('fs', 'tp'), may hold values from -0.125 to 0.125
- w_up: bfloat16 [2048, 3072], P('fs', 'tp'), may hold values from -0.125 to 0.125
- w_down: bfloat16 [3072, 2048], P('tp', 'fs'), may hold values from -0.109375 to 0.109375
- post_gain: float32 [2048], replicated, may hold values from 0.1 to 1.9
Outputs:
- result: bfloat16 [4096, 2048], P(('rep', 'fs', 'tp'))
All inputs are finite; a program needn't handle non-finite values.
Results may differ from a plain program's by a relative error of at most 0.014.
Values may be sent and summed in bfloat16 or wider, within the bound.
A program may use at most 64 MiB of HBM per device.

v0:
```python
import jax
import jax.numpy as jnp
from jax import lax
from jax.sharding import PartitionSpec as P

EPS = 1e-06


def rms_scale(values, gain):
    return values * lax.rsqrt(jnp.mean(values * values, axis=-1, keepdims=True) + EPS) * gain


def body(tokens, norm_gain, w_gate, w_up, w_down, post_gain):
    own_normed = rms_scale(tokens.astype(jnp.float32), norm_gain).astype(jnp.bfloat16)
    normed = lax.all_gather(own_normed, "tp", axis=0, tiled=True)
    gate = jnp.dot(
        normed, lax.all_gather(w_gate, "fs", axis=0, tiled=True), preferred_element_type=jnp.float32
    )
    up = jnp.dot(
        normed, lax.all_gather(w_up, "fs", axis=0, tiled=True), preferred_element_type=jnp.float32
    )
    hidden = (jax.nn.silu(gate) * up).astype(jnp.bfloat16)
    terms = jnp.dot(
        hidden, lax.all_gather(w_down, "fs", axis=1, tiled=True), preferred_element_type=jnp.float32
    )
    summed = lax.psum_scatter(
        terms.astype(jnp.bfloat16), "tp", scatter_dimension=0, tiled=True
    ).astype(jnp.float32)
    return rms_scale(summed, post_gain).astype(jnp.bfloat16)


def solution(mesh):
    return jax.shard_map(
        body,
        mesh=mesh,
        in_specs=(
            P(("rep", "fs", "tp"), None),
            P(),
            P("fs", "tp"),
            P("fs", "tp"),
            P("tp", "fs"),
            P(),
        ),
        out_specs=P(("rep", "fs", "tp"), None),
        check_vma=False,
    )
```

profile of v0, /device:TPU:0, one launch (start us, length us, event | category | flops | bytes accessed | tf_op | source)
XLA Modules:
  0.0 276.0 jit_solution(9713884520916390494)
XLA Ops:
  6.5 0.0 all-gather.5.cloned.1.call-start
  6.5 1.2 fusion
  7.8 2.0 fusion.2
  9.8 0.0 all-gather.5.cloned.1.call-update
  9.8 0.0 all-gather.7.cloned.1.call-start
  9.9 0.7 all-gather.7.cloned.1.call-update
  10.6 0.0 all-gather.11.cloned.1.call-start
  10.6 0.7 all-gather.11.cloned.1.call-update
  11.3 0.0 all-gather.9.cloned.1.call-start
  11.4 0.5 all-gather.9.cloned.1.call-update
  11.9 0.0 reduce-scatter.2.cloned.1.call-start
  11.9 23.3 %all-gather.5.cloned.1.call-done = bf16[512,2048]{1,0:T(8,128)(2,1)} async-done(((bf16[128,2048]{1,0:T(8,128)(2,1)}), bf16[512,2048]{1,0:T(8,128)(2,1)}) %all-gather.5.cloned.1.call-update) | async-done | bytes 2097168 | tf_op jit(solution)/shard_map/all_gather | solution.py:15
  35.3 0.0 copy-start.1
  35.3 65.0 %all-gather.7.cloned.1.call-done = bf16[2048,768]{1,0:T(8,128)(2,1)} async-done(((bf16[512,768]{1,0:T(8,128)(2,1)}), bf16[2048,768]{1,0:T(8,128)(2,1)}) %all-gather.7.cloned.1.call-update) | async-done | bytes 3145744 | tf_op jit(solution)/shard_map/all_gather | solution.py:17
  100.3 5.5 %fusion.7 = f32[512,768]{1,0:T(8,128)} fusion(bf16[512,2048]{1,0:T(8,128)(2,1)} %all-gather.5.cloned.1.call-done, bf16[2048,768]{1,0:T(8,128)(2,1)} %all-gather.7.cloned.1.call-done), kind=kOutput, calls=%fused_computation.15 | convolution fusion | flops 1610612736 | bytes 6815744 | tf_op jit(solution)/shard_map/dot_general | solution.py:16
  105.8 58.2 %all-gather.11.cloned.1.call-done = bf16[768,2048]{1,0:T(8,128)(2,1)} async-done(((bf16[768,512]{1,0:T(8,128)(2,1)}), bf16[768,2048]{1,0:T(8,128)(2,1)}) %all-gather.11.cloned.1.call-update) | async-done | bytes 3145744 | tf_op jit(solution)/shard_map/all_gather | solution.py:24
  164.0 63.5 %all-gather.9.cloned.1.call-done = bf16[2048,768]{1,0:T(8,128)(2,1)} async-done(((bf16[512,768]{1,0:T(8,128)(2,1)}), bf16[2048,768]{1,0:T(8,128)(2,1)}) %all-gather.9.cloned.1.call-update) | async-done | bytes 3145744 | tf_op jit(solution)/shard_map/all_gather | solution.py:20
  227.5 0.0 copy-done.1
  227.6 8.6 %convolution_convert_fusion = bf16[512,2048]{1,0:T(8,128)(2,1)} fusion(bf16[768,2048]{1,0:T(8,128)(2,1)} %all-gather.11.cloned.1.call-done, f32[512,768]{1,0:T(8,128)} %fusion.7, bf16[512,2048]{1,0:T(8,128)(2,1)S(1)} %copy-done.1, bf16[2048,768]{1,0:T(8,128)(2,1)} %all-gather.9.cloned.1.call-done), kind=kOutput, calls=%fused_computation | convolution fusion | flops 3224633344 | bytes 12058624 | tf_op jit(solution)/shard_map/dot_general | solution.py:23
  236.2 0.0 copy-start
  236.2 0.0 reduce-scatter.2.cloned.1.call-update
  236.2 30.0 %reduce-scatter.2.cloned.1.call-done = bf16[128,2048]{1,0:T(8,128)(2,1)} async-done(((bf16[512,2048]{1,0:T(8,128)(2,1)}), bf16[128,2048]{1,0:T(8,128)(2,1)}) %reduce-scatter.2.cloned.1.call-update) | async-done | bytes 524304 | tf_op jit(solution)/shard_map/reduce_scatter | solution.py:26
  266.2 1.2 fusion.3
  267.4 0.0 copy-done
  267.4 2.0 fusion.5
  (2 shorter events, 0.0 us)
Async XLA Ops:
  6.5 28.7 %all-gather.5.cloned.1.call-start = ((), (), s32[]{:S(2)}) async-start(), calls=%async_computation.1 | async-start | bytes 2621440 | tf_op jit(solution)/shard_map/all_gather | solution.py:15
  9.8 90.5 %all-gather.7.cloned.1.call-start = ((), (), s32[]{:S(2)}) async-start(), calls=%async_computation.2 | async-start | bytes 3932160 | tf_op jit(solution)/shard_map/all_gather | solution.py:17
  10.6 153.4 %all-gather.11.cloned.1.call-start = ((), (), s32[]{:S(2)}) async-start(), calls=%async_computation.4 | async-start | bytes 3932160 | tf_op jit(solution)/shard_map/all_gather | solution.py:24
  11.3 216.2 %all-gather.9.cloned.1.call-start = ((), (), s32[]{:S(2)}) async-start(), calls=%async_computation.3 | async-start | bytes 3932160 | tf_op jit(solution)/shard_map/all_gather | solution.py:20
  11.9 254.3 %reduce-scatter.2.cloned.1.call-start = ((), (), s32[]{:S(2)}) async-start(), calls=%async_computation.5 | async-start | bytes 2621440 | tf_op jit(solution)/shard_map/reduce_scatter | solution.py:26
  35.3 192.3 %copy-start.1 = (bf16[512,2048]{1,0:T(8,128)(2,1)S(1)}, bf16[512,2048]{1,0:T(8,128)(2,1)}, u32[]{:S(2)}) copy-start(bf16[512,2048]{1,0:T(8,128)(2,1)} %all-gather.5.cloned.1.call-done) | copy-start | bytes 6291460
  236.2 31.2 %copy-start = (f32[2048]{0:T(1024)S(1)}, f32[2048]{0:T(1024)}, u32[]{:S(2)}) copy-start(f32[2048]{0:T(1024)} %param.11) | copy-start | bytes 24580
Sparse Core Ops, SparseCore 0:
  9.9 25.2 all-gather.4
  36.8 63.4 all-gather.6
  101.9 62.0 all-gather.10
  165.4 62.0 all-gather.8
  236.3 29.7 reduce-scatter.1
where the time goes:
time: 276 us
  waiting for transfers between devices  242 us (88%)
  matrix products  14.1 us (5%)
  between operations  13.1 us (5%)
  other arithmetic  6.53 us (2%)
    all_gather x1, waiting for transfers between devices, body(): lax.all_gather(w_gate, 'fs', axis=0, tiled=True)  65 us
    all_gather x1, waiting for transfers between devices, body(): lax.all_gather(w_up, 'fs', axis=0, tiled=True)  63.5 us
    all_gather x1, waiting for transfers between devices, body(): lax.all_gather(w_down, 'fs', axis=1, tiled=True)  58.2 us
    reduce_scatter x1, waiting for transfers between devices, body(): lax.psum_scatter(terms.astype(jnp.bfloat16), 'tp', scatter_dimension=0, t...  30 us
    all_gather x1, waiting for transfers between devices, body(): normed = lax.all_gather(own_normed, 'tp', axis=0, tiled=True)  23.3 us
    dot_general x1, matrix products, body(): jnp.dot(hidden, lax.all_gather(w_down, 'fs', axis=1, tiled=True), preferr...  8.63 us
  transfers between devices with their start and end apart: 5, of which 5 were waited for; matrix products, arithmetic and copies ran while one was open for 2% of the time, Pallas kernels for 0%

commit v1 on v0

--- a/solution.py
+++ b/solution.py
@@ -12,7 +12,12 @@
 
 def body(tokens, norm_gain, w_gate, w_up, w_down, post_gain):
     own_normed = rms_scale(tokens.astype(jnp.float32), norm_gain).astype(jnp.bfloat16)
-    normed = lax.all_gather(own_normed, "tp", axis=0, tiled=True)
+    ring = [own_normed]
+    for hop in range(3):
+        ring.append(lax.ppermute(ring[-1], "tp", [(dev, (dev + 1) % 4) for dev in range(4)]))
+    normed = jnp.roll(
+        jnp.concatenate(ring[::-1], axis=0), (lax.axis_index("tp") + 1) * ring[0].shape[0], axis=0
+    )
     gate = jnp.dot(
         normed, lax.all_gather(w_gate, "fs", axis=0, tiled=True), preferred_element_type=jnp.float32
     )

time: 276 us -> 251 us (0.909)
  waiting for transfers between devices: 242 us -> 212 us
  local copies, waits for them, and re-layouts: 0.01 us -> 5.03 us
    all_gather x1, waiting for transfers between devices: 63.5 us -> 30.7 us  [body(): lax.all_gather(w_up, 'fs', axis=0, tiled=True)]
    ppermute x0 -> x3, waiting for transfers between devices: none -> 26 us  [body(): lax.ppermute(ring[-1], 'tp', [(dev, (dev + 1) % 4) for dev in range(4)])]
    all_gather x1 -> x0, waiting for transfers between devices: 23.3 us -> none  [body(): normed = lax.all_gather(own_normed, 'tp', axis=0, tiled=True)]
    all_gather x1, waiting for transfers between devices: 65 us -> 59.4 us  [body(): lax.all_gather(w_gate, 'fs', axis=0, tiled=True)]
    all_gather x1, waiting for transfers between devices: 58.2 us -> 63.7 us  [body(): lax.all_gather(w_down, 'fs', axis=1, tiled=True)]
    unnamed x4 -> x12, local copies, waits for them, and re-layouts: 0.01 us -> 5.03 us
  transfers between devices with their start and end apart: 5 -> 7, of which waited for: 5 -> 7; matrix products, arithmetic and copies ran while one was open for 2% -> 5% of each run, Pallas kernels for 0% -> 0%
where the time goes in v1:
time: 251 us
  waiting for transfers between devices  212 us (84%)
  between operations  13.2 us (5%)
  matrix products  13.1 us (5%)
  other arithmetic  7.33 us (3%)
  local copies, waits for them, and re-layouts  5.03 us (2%)
    all_gather x1, waiting for transfers between devices, body(): lax.all_gather(w_down, 'fs', axis=1, tiled=True)  63.7 us
    all_gather x1, waiting for transfers between devices, body(): lax.all_gather(w_gate, 'fs', axis=0, tiled=True)  59.4 us
    all_gather x1, waiting for transfers between devices, body(): lax.all_gather(w_up, 'fs', axis=0, tiled=True)  30.7 us
    reduce_scatter x1, waiting for transfers between devices, body(): lax.psum_scatter(terms.astype(jnp.bfloat16), 'tp', scatter_dimension=0, t...  30 us
    ppermute x3, waiting for transfers between devices, body(): lax.ppermute(ring[-1], 'tp', [(dev, (dev + 1) % 4) for dev in range(4)])  26 us
    dot_general x1, matrix products, body(): jnp.dot(hidden, lax.all_gather(w_down, 'fs', axis=1, tiled=True), preferr...  8.82 us
    unnamed x12, local copies, waits for them, and re-layouts  5.03 us
  transfers between devices with their start and end apart: 7, of which 7 were waited for; matrix products, arithmetic and copies ran while one was open for 5% of the time, Pallas kernels for 0%

profile of v1, /device:TPU:0, one launch (start us, length us, event | category | flops | bytes accessed | tf_op | source)
XLA Modules:
  0.0 251.1 jit_solution(12599917524785784371)
XLA Ops:
  6.5 0.0 copy-start
  6.5 0.0 all-gather.6.cloned.1.call-start
  6.5 0.7 all-gather.6.cloned.1.call-update
  7.3 0.0 copy-start.1
  7.3 0.0 all-gather.4.cloned.1.call-start
  7.3 0.7 all-gather.4.cloned.1.call-update
  8.0 0.0 all-gather.8.cloned.1.call-start
  8.1 0.7 all-gather.8.cloned.1.call-update
  8.8 0.0 reduce-scatter.2.cloned.1.call-start
  8.8 1.2 fusion.4
  10.0 0.0 copy-done
  10.0 0.9 fusion.6
  10.9 0.5 collective-permute-start
  11.5 8.8 %collective-permute-done = bf16[128,2048]{1,0:T(8,128)(2,1)S(1)} collective-permute-done((bf16[128,2048]{1,0:T(8,128)(2,1)S(1)}, bf16[128,2048]{1,0:T(8,128)(2,1)S(1)}, u32[]{:S(2)}, u32[]{:S(2)}) %collective-permute-start) | collective-permute-done | bytes 524320 | tf_op jit(solution)/shard_map/ppermute | solution.py:17
  20.3 0.0 collective-permute-start.1
  20.3 8.6 %collective-permute-done.1 = bf16[128,2048]{1,0:T(8,128)(2,1)S(1)} collective-permute-done((bf16[128,2048]{1,0:T(8,128)(2,1)S(1)}, bf16[128,2048]{1,0:T(8,128)(2,1)S(1)}, u32[]{:S(2)}, u32[]{:S(2)}) %collective-permute-start.1) | collective-permute-done | bytes 524320 | tf_op jit(solution)/shard_map/ppermute | solution.py:17
  28.9 0.0 collective-permute-start.2
  28.9 8.6 %collective-permute-done.2 = bf16[128,2048]{1,0:T(8,128)(2,1)S(1)} collective-permute-done((bf16[128,2048]{1,0:T(8,128)(2,1)S(1)}, bf16[128,2048]{1,0:T(8,128)(2,1)S(1)}, u32[]{:S(2)}, u32[]{:S(2)}) %collective-permute-start.2) | collective-permute-done | bytes 524320 | tf_op jit(solution)/shard_map/ppermute | solution.py:17
  37.5 0.8 constant_dynamic-update-slice_fusion.7
  38.3 0.8 constant_dynamic-update-slice_fusion.6
  39.1 0.9 constant_dynamic-update-slice_fusion.5
  40.0 0.0 copy-done.1
  40.0 1.0 constant_dynamic-update-slice_fusion.4
  41.0 0.8 constant_dynamic-update-slice_fusion.3
  41.8 0.8 constant_dynamic-update-slice_fusion.2
  42.6 0.8 constant_dynamic-update-slice_fusion.1
  43.5 1.0 constant_dynamic-update-slice_fusion
  44.4 30.7 %all-gather.6.cloned.1.call-done = bf16[2048,768]{1,0:T(8,128)(2,1)} async-done(((bf16[512,768]{1,0:T(8,128)(2,1)}), bf16[2048,768]{1,0:T(8,128)(2,1)}) %all-gather.6.cloned.1.call-update) | async-done | bytes 3145744 | tf_op jit(solution)/shard_map/all_gather | solution.py:25
  75.1 4.3 %fusion = f32[512,768]{1,0:T(8,128)S(1)} fusion(bf16[2048,768]{1,0:T(8,128)(2,1)} %all-gather.6.cloned.1.call-done, bf16[1024,2048]{1,0:T(8,128)(2,1)} %constant_dynamic-update-slice_fusion, s32[]{:T(128)S(6)} %select_n.14), kind=kOutput, calls=%fused_computation.1 | convolution fusion | flops 1610612736 | bytes 6815748 | tf_op jit(solution)/shard_map/dot_general | solution.py:24
  79.4 0.0 copy-start.2
  79.4 59.4 %all-gather.4.cloned.1.call-done = bf16[2048,768]{1,0:T(8,128)(2,1)} async-done(((bf16[512,768]{1,0:T(8,128)(2,1)}), bf16[2048,768]{1,0:T(8,128)(2,1)}) %all-gather.4.cloned.1.call-update) | async-done | bytes 3145744 | tf_op jit(solution)/shard_map/all_gather | solution.py:22
  138.8 63.7 %all-gather.8.cloned.1.call-done = bf16[768,2048]{1,0:T(8,128)(2,1)} async-done(((bf16[768,512]{1,0:T(8,128)(2,1)}), bf16[768,2048]{1,0:T(8,128)(2,1)}) %all-gather.8.cloned.1.call-update) | async-done | bytes 3145744 | tf_op jit(solution)/shard_map/all_gather | solution.py:29
  202.5 8.8 %convolution_convert_fusion = bf16[512,2048]{1,0:T(8,128)(2,1)} fusion(bf16[768,2048]{1,0:T(8,128)(2,1)} %all-gather.8.cloned.1.call-done, f32[512,768]{1,0:T(8,128)S(1)} %fusion, bf16[2048,768]{1,0:T(8,128)(2,1)} %all-gather.4.cloned.1.call-done, bf16[1024,2048]{1,0:T(8,128)(2,1)} %constant_dynamic-update-slice_fusion, s32[]{:T(128)S(6)} %select_n.14), kind=kOutput, calls=%fused_computation | convolution fusion | flops 3224633344 | bytes 12058628 | tf_op jit(solution)/shard_map/dot_general | solution.py:28
  211.3 0.0 reduce-scatter.2.cloned.1.call-update
  211.3 30.0 %reduce-scatter.2.cloned.1.call-done = bf16[128,2048]{1,0:T(8,128)(2,1)} async-done(((bf16[512,2048]{1,0:T(8,128)(2,1)}), bf16[128,2048]{1,0:T(8,128)(2,1)}) %reduce-scatter.2.cloned.1.call-update) | async-done | bytes 524304 | tf_op jit(solution)/shard_map/reduce_scatter | solution.py:31
  241.3 1.2 fusion.7
  242.5 0.0 copy-done.2
  242.6 2.0 fusion.9
  (2 shorter events, 0.0 us)
Async XLA Ops:
  6.5 3.5 %copy-start = (bf16[128,2048]{1,0:T(8,128)(2,1)S(1)}, bf16[128,2048]{1,0:T(8,128)(2,1)}, u32[]{:S(2)}) copy-start(bf16[128,2048]{1,0:T(8,128)(2,1)} %param.6) | copy-start | bytes 1572868
  6.5 68.6 %all-gather.6.cloned.1.call-start = ((), (), s32[]{:S(2)}) async-start(), calls=%async_computation.2 | async-start | bytes 3932160 | tf_op jit(solution)/shard_map/all_gather | solution.py:25
  7.3 32.7 %copy-start.1 = (f32[2048]{0:T(1024)S(1)}, f32[2048]{0:T(1024)}, u32[]{:S(2)}) copy-start(f32[2048]{0:T(1024)} %param.7) | copy-start | bytes 24580
  7.3 131.5 %all-gather.4.cloned.1.call-start = ((), (), s32[]{:S(2)}) async-start(), calls=%async_computation.1 | async-start | bytes 3932160 | tf_op jit(solution)/shard_map/all_gather | solution.py:22
  8.0 194.5 %all-gather.8.cloned.1.call-start = ((), (), s32[]{:S(2)}) async-start(), calls=%async_computation.3 | async-start | bytes 3932160 | tf_op jit(solution)/shard_map/all_gather | solution.py:29
  8.8 232.6 %reduce-scatter.2.cloned.1.call-start = ((), (), s32[]{:S(2)}) async-start(), calls=%async_computation.4 | async-start | bytes 2621440 | tf_op jit(solution)/shard_map/reduce_scatter | solution.py:31
  10.9 9.3 %collective-permute-start = (bf16[128,2048]{1,0:T(8,128)(2,1)S(1)}, bf16[128,2048]{1,0:T(8,128)(2,1)S(1)}, u32[]{:S(2)}, u32[]{:S(2)}) collective-permute-start(bf16[128,2048]{1,0:T(8,128)(2,1)S(1)} %fusion.6), channel_id=1, source_target_pairs={{0,1},{1,2},{2,3},{3,0},{4,5},{5,6},{6,7},{7,4},{8,9},{9,10},{10,1... | collective-permute-start | bytes 1572872 | tf_op jit(solution)/shard_map/ppermute | solution.py:17
  20.3 8.6 %collective-permute-start.1 = (bf16[128,2048]{1,0:T(8,128)(2,1)S(1)}, bf16[128,2048]{1,0:T(8,128)(2,1)S(1)}, u32[]{:S(2)}, u32[]{:S(2)}) collective-permute-start(bf16[128,2048]{1,0:T(8,128)(2,1)S(1)} %collective-permute-done), channel_id=1, source_target_pairs={{0,1},{1,2},{2,3},{3,0},{4,5},{5,6},{6,7},{7,4},{8,9},{9,10},{10,1... | collective-permute-start | bytes 1572872 | tf_op jit(solution)/shard_map/ppermute | solution.py:17
  28.9 8.6 %collective-permute-start.2 = (bf16[128,2048]{1,0:T(8,128)(2,1)S(1)}, bf16[128,2048]{1,0:T(8,128)(2,1)S(1)}, u32[]{:S(2)}, u32[]{:S(2)}) collective-permute-start(bf16[128,2048]{1,0:T(8,128)(2,1)S(1)} %collective-permute-done.1), channel_id=1, source_target_pairs={{0,1},{1,2},{2,3},{3,0},{4,5},{5,6},{6,7},{7,4},{8,9},{9,10},{10,1... | collective-permute-start | bytes 1572872 | tf_op jit(solution)/shard_map/ppermute | solution.py:17
  79.4 163.1 %copy-start.2 = (f32[2048]{0:T(1024)S(1)}, f32[2048]{0:T(1024)}, u32[]{:S(2)}) copy-start(f32[2048]{0:T(1024)} %param.11) | copy-start | bytes 24580
Sparse Core Ops, SparseCore 0:
  8.9 66.1 all-gather.5
  76.7 62.0 all-gather.3
  140.4 62.0 all-gather.7
  211.4 29.8 reduce-scatter.1
